TPU v7x, 32 devices: a whole 2x2x4 slice. The times are simulated.
32 devices in a mesh: sp: 8 (over z, x), tp: 4 (over y, core).
Axes of the slice: x: 2, y: 2, z: 4, core: 2. Of those that a mesh axis runs over, the one named last changes fastest.
Arguments:
- inputs: bfloat16 [8192, 2048], P('sp'), may hold values from -9 to 9
- w_query: bfloat16 [2048, 1024], P(None, 'tp'), may hold values from -0.15692044 to 0.15692044
- w_key: bfloat16 [2048, 1024], P(None, 'tp'), may hold values from -0.15692044 to 0.15692044
- w_value: bfloat16 [2048, 1024], P(None, 'tp'), may hold values from -0.125 to 0.125
- w_glu_value: bfloat16 [2048, 1024], P(None, 'tp'), may hold values from -0.37565048 to 0.37565048
- w_glu_gate: bfloat16 [2048, 1024], P(None, 'tp'), may hold values from -0.125 to 0.125
- conv_taps: float32 [31, 1024], P(None, 'tp'), may hold values from -4 to 4
- conv_gain: float32 [1024], P('tp'), may hold values from 0.1 to 1.9
- log_forget: float32 [8192, 8], P('sp', 'tp'), may hold values from -8192 to 0, as said below
- w_out: bfloat16 [2048, 2048], replicated, may hold values from -0.125 to 0.125
Outputs:
- result: bfloat16 [8192, 2048], P(('sp', 'tp'))
Inputs may be any that keep to these rules, and one draw needn't show every extreme that they name: `log_forget`: for each head, non-increasing along positions and at most zero.
All inputs are finite; a program needn't handle non-finite values.
Results may differ from a plain program's by a relative error of at most 0.014.
Values may be sent and summed in bfloat16 or wider, within the bound.
A program may use at most 128 MiB of HBM per device.

v0:
```python
import math
import jax
import jax.numpy as jnp
from jax import lax
from jax.sharding import PartitionSpec as P

HEAD_DIM = 128
NORM_EPS = 1e-05


def passed_along(value, axis, steps):
    count = lax.axis_size(axis)
    leading, last = (max(0, -steps), min(count, count - steps))
    return lax.ppermute(value, axis, [(source, source + steps) for source in range(leading, last)])


def on_device(
    inputs,
    w_query,
    w_key,
    w_value,
    w_glu_value,
    w_glu_gate,
    conv_taps,
    conv_gain,
    log_forget,
    w_out,
):
    tok_rows = inputs.shape[0]
    channels = w_glu_value.shape[1]
    heads_here = w_query.shape[1] // HEAD_DIM
    attn_width = heads_here * HEAD_DIM
    tp_count = lax.axis_size("tp")
    tp_place = lax.axis_index("tp")
    total_channels = channels * tp_count
    row_start = lax.axis_index("sp") * tok_rows
    last_row = row_start + tok_rows - 1
    glu_value = jnp.dot(inputs, w_glu_value, preferred_element_type=jnp.float32)
    glu_gate = jnp.dot(inputs, w_glu_gate, preferred_element_type=jnp.float32)
    gated = (glu_value * jax.nn.sigmoid(glu_gate)).astype(jnp.bfloat16)
    kernel = conv_taps.shape[0]
    halo_rows = passed_along(gated[tok_rows - (kernel - 1) :], "sp", 1)
    padded = jnp.concatenate([halo_rows, gated], axis=0).astype(jnp.float32)
    conv_sum = jnp.zeros((tok_rows, channels), jnp.float32)
    for offset in range(kernel):
        conv_sum = conv_sum + conv_taps[offset] * padded[offset : offset + tok_rows]
    mean_value = lax.psum(jnp.sum(conv_sum, axis=1), "tp") / total_channels
    centered = conv_sum - mean_value[:, None]
    spread = lax.psum(jnp.sum(centered * centered, axis=1), "tp") / total_channels
    conv_rows = jax.nn.silu(centered * lax.rsqrt(spread + NORM_EPS)[:, None] * conv_gain).astype(
        jnp.bfloat16
    )
    query_rows = jnp.dot(inputs, w_query, preferred_element_type=jnp.float32).astype(jnp.bfloat16)
    key_rows = jnp.dot(inputs, w_key, preferred_element_type=jnp.float32).astype(jnp.bfloat16)
    value_rows = jnp.dot(inputs, w_value, preferred_element_type=jnp.float32).astype(jnp.bfloat16)
    query_heads = query_rows.reshape(tok_rows, heads_here, HEAD_DIM)
    own_gates = jnp.transpose(log_forget)
    gates_all = lax.all_gather(log_forget, "sp", axis=0, tiled=True)
    score_scale = HEAD_DIM ** (-0.5)
    query_pos = row_start + jnp.arange(tok_rows, dtype=jnp.int32)
    start_state = (
        jnp.full((heads_here, tok_rows), -1e30, jnp.float32),
        jnp.zeros((heads_here, tok_rows), jnp.float32),
        jnp.zeros((heads_here, tok_rows, HEAD_DIM), jnp.float32),
    )
    piece_keys = lax.all_gather(key_rows, "sp", axis=0, tiled=True)
    piece_values = lax.all_gather(value_rows, "sp", axis=0, tiled=True)
    block_rows = math.gcd(piece_keys.shape[0], tok_rows)
    shards = piece_keys.shape[0] // block_rows
    key_iota = jnp.arange(block_rows, dtype=jnp.int32)

    def one_shard(shard_number, carried_state):
        offset = shard_number * block_rows
        key_first = offset

        def attend(state_in):
            running_max, running_sum, running_out = state_in
            shard_keys = lax.dynamic_slice_in_dim(piece_keys, offset, block_rows, 0).reshape(
                block_rows, heads_here, HEAD_DIM
            )
            shard_values = lax.dynamic_slice_in_dim(piece_values, offset, block_rows, 0).reshape(
                block_rows, heads_here, HEAD_DIM
            )
            shard_gates = jnp.transpose(
                lax.dynamic_slice_in_dim(gates_all, key_first, block_rows, 0)
            )
            scores = (
                jnp.einsum(
                    "qhd,khd->hqk", query_heads, shard_keys, preferred_element_type=jnp.float32
                )
                * score_scale
            )
            scores = scores + own_gates[:, :, None] - shard_gates[:, None, :]
            allowed = ((key_first + key_iota)[None, :] <= query_pos[:, None])[None]
            masked = jnp.where(allowed, scores, -1e30)
            new_max = jnp.maximum(running_max, jnp.max(masked, axis=2))
            weights = jnp.where(allowed, jnp.exp(masked - new_max[:, :, None]), 0.0)
            rescale = jnp.exp(running_max - new_max)
            new_sum = running_sum * rescale + jnp.sum(weights, axis=2)
            mixture = jnp.einsum(
                "hqk,khd->hqd",
                weights.astype(jnp.bfloat16),
                shard_values,
                preferred_element_type=jnp.float32,
            )
            new_out = running_out * rescale[:, :, None] + mixture
            return (new_max, new_sum, new_out)

        def keep_state(state_in):
            return state_in

        return lax.cond(key_first <= last_row, attend, keep_state, carried_state)

    final_max, final_sum, final_out = lax.fori_loop(0, shards, one_shard, start_state)
    attn_heads = (final_out / final_sum[:, :, None]).astype(jnp.bfloat16)
    attn_rows = jnp.transpose(attn_heads, (1, 0, 2)).reshape(tok_rows, attn_width)
    conv_weight = lax.dynamic_slice_in_dim(w_out, tp_place * channels, channels, 0)
    attn_weight = lax.dynamic_slice_in_dim(
        w_out, total_channels + tp_place * attn_width, attn_width, 0
    )
    projected = jnp.dot(conv_rows, conv_weight, preferred_element_type=jnp.float32)
    return lax.psum_scatter(
        (projected + jnp.dot(attn_rows, attn_weight, preferred_element_type=jnp.float32)).astype(
            jnp.bfloat16
        ),
        "tp",
        scatter_dimension=0,
        tiled=True,
    )


def solution(mesh):
    in_specs = (
        P("sp", None),
        P(None, "tp"),
        P(None, "tp"),
        P(None, "tp"),
        P(None, "tp"),
        P(None, "tp"),
        P(None, "tp"),
        P("tp"),
        P("sp", "tp"),
        P(),
    )
    out_specs = P(("sp", "tp"), None)
    return jax.shard_map(
        on_device, mesh=mesh, in_specs=in_specs, out_specs=out_specs, check_vma=False
    )
```

profile of v0, /device:TPU:0, one launch (start us, length us, event | category | flops | bytes accessed | tf_op | source)
XLA Modules:
  0.0 321.7 jit_solution(7589455608530308768)
XLA Ops:
  6.5 0.0 copy-start
  6.5 0.0 copy-start.6
  6.5 0.0 all-gather.3.cloned.1.call-start
  6.5 1.2 copy-done
  7.8 4.2 %convolution_convert_fusion.2 = bf16[1024,256]{1,0:T(8,128)(2,1)} fusion(bf16[1024,2048]{1,0:T(8,128)(2,1)} %param.14, bf16[2048,256]{1,0:T(8,128)(2,1)S(1)} %copy-done), kind=kOutput, calls=%fused_computation.30 | convolution fusion | flops 1074003968 | bytes 5767168 | tf_op jit(solution)/shard_map/dot_general | solution.py:54
  12.0 0.0 all-gather.3.cloned.1.call-update
  12.0 0.0 copy-start.7
  12.0 0.0 all-gather.5.cloned.1.call-start
  12.1 4.6 %convolution_convert_fusion = bf16[1024,256]{1,0:T(8,128)(2,1)} fusion(bf16[1024,2048]{1,0:T(8,128)(2,1)} %param.14, bf16[2048,256]{1,0:T(8,128)(2,1)} %param.17), kind=kOutput, calls=%fused_computation.28 | convolution fusion | flops 1074003968 | bytes 5767168 | tf_op jit(solution)/shard_map/dot_general | solution.py:55
  16.7 0.0 all-gather.5.cloned.1.call-update
  16.7 0.0 reduce-scatter.2.cloned.1.call-start
  16.8 0.0 copy-done.6
  16.8 0.0 copy-start.5
  16.8 3.6 %fusion.18 = f32[1024,256]{1,0:T(8,128)S(1)} fusion(bf16[1024,2048]{1,0:T(8,128)(2,1)} %param.14, bf16[2048,256]{1,0:T(8,128)(2,1)S(1)} %copy-done.6), kind=kOutput, calls=%fused_computation.26 | convolution fusion | flops 1074528256 | bytes 6291456 | tf_op jit(solution)/shard_map/dot_general | solution.py:39
  20.4 0.0 copy-done.7
  20.4 0.0 copy-done.5
  20.4 1.3 fusion.19
  21.7 0.0 copy-start.3
  21.7 0.0 copy-start.2
  21.7 4.9 %collective-permute-start = (bf16[30,256]{1,0:T(8,128)(2,1)S(1)}, bf16[30,256]{1,0:T(8,128)(2,1)S(1)}, u32[]{:S(2)}, u32[]{:S(2)}) collective-permute-start(bf16[30,256]{1,0:T(8,128)(2,1)S(1)} %slice.252), channel_id=1, source_target_pairs={{0,4},{4,8},{8,12},{12,16},{16,20},{20,24},{24,28},{1,5},{5,9},{9,... | collective-permute-start | bytes 46088 | tf_op jit(solution)/shard_map/ppermute | solution.py:14
  26.6 3.8 %convolution_convert_fusion.1 = bf16[1024,256]{0,1:T(8,128)(2,1)S(1)} fusion(bf16[1024,2048]{1,0:T(8,128)(2,1)} %param.14, bf16[2048,256]{1,0:T(8,128)(2,1)} %param.15), kind=kOutput, calls=%fused_computation.29 | convolution fusion | flops 1074003968 | bytes 5767168 | tf_op jit(solution)/shard_map/dot_general | solution.py:53
  30.4 0.3 copy.17
  30.7 0.0 copy-done.3
  30.8 0.0 copy-done.2
  30.8 31.8 %all_gather.10 = f32[8192,2]{0,1:T(2,128)S(1)} all-gather(f32[1024,2]{0,1:T(2,128)S(1)} %copy-done.2), channel_id=1, replica_groups=mesh['sp'=8,'tp'=4] {'sp'}, dimensions={0}, use_global_device_ids=true | all-gather | bytes 73728 | tf_op jit(solution)/shard_map/all_gather | solution.py:58
  62.6 0.0 collective-permute-done
  62.6 0.1 maximum_convert_fusion
  62.7 0.0 copy-start.4
  62.7 4.3 %fusion.60 = (f32[1024]{0:T(1024)S(1)}, f32[1024,256]{1,0:T(8,128)S(1)}) fusion(f32[1054,256]{1,0:T(8,128)S(1)} %maximum_convert_fusion, f32[256]{0:T(256)S(1)} %bitcast.80, f32[256]{0:T(256)S(1)} %bitcast.81, f32[256]{0:T(256)S(1)} %bitcast.83, f32[256]{0:T(256)S(1)} %bitcast.84, f32[256]{0:T(256)S(1)} %bitcast.85, f32[256]{0:T(256)S(1)} %bitcast.86, ...), kind=kLoop, calls=%fused_computation.108 | loop fusion | flops 16251904 | bytes 33590272 | tf_op jit(solution)/shard_map/reduce_sum | solution.py:47
  67.1 6.1 %psum.14 = f32[1024]{0:T(1024)S(1)} all-reduce(f32[1024]{0:T(1024)S(1)} %get-tuple-element.333), channel_id=1, replica_groups=mesh['sp'=8,'tp'=4] {'tp'}, use_global_device_ids=true, to_apply=%region_1.0 | all-reduce | flops 1024 | bytes 8192 | tf_op jit(solution)/shard_map/psum | solution.py:47
  73.2 0.4 multiply_reduce_fusion
  73.5 6.6 %psum.15 = f32[1024]{0:T(1024)S(1)} all-reduce(f32[1024]{0:T(1024)S(1)} %multiply_reduce_fusion), channel_id=1, replica_groups=mesh['sp'=8,'tp'=4] {'tp'}, use_global_device_ids=true, to_apply=%region_3.0 | all-reduce | flops 1024 | bytes 8192 | tf_op jit(solution)/shard_map/psum | solution.py:49
  80.2 0.0 copy-done.4
  80.2 5.8 %fusion.51 = f32[1024,2048]{1,0:T(8,128)} fusion(bf16[2048,2048]{1,0:T(8,128)(2,1)} %param.23, s32[]{:T(128)S(6)} %select_n.18, f32[1024,256]{1,0:T(8,128)S(1)} %get-tuple-element.334, f32[256]{0:T(256)S(1)} %copy-done.4, f32[1024]{0:T(1024)S(1)} %add_rsqrt_fusion, f32[1024]{0:T(1024)S(1)} %broadcast_multiply_fusion), kind=kOutput, calls=%fused_computation.94 | convolution fusion | flops 1075838976 | bytes 10494980 | tf_op jit(solution)/shard_map/dot_general | solution.py:121
  86.0 2.5 all-gather.3.cloned.1.call-done
  88.5 6.4 %copy.16 = bf16[8192,256]{0,1:T(8,128)(2,1)} copy(bf16[8192,256]{1,0:T(8,128)(2,1)} %all-gather.3.cloned.1.call-done) | data formatting | bytes 8388608
  94.9 67.2 %all-gather.5.cloned.1.call-done = bf16[8192,256]{1,0:T(8,128)(2,1)} async-done(((bf16[1024,256]{1,0:T(8,128)(2,1)}), bf16[8192,256]{1,0:T(8,128)(2,1)}) %all-gather.5.cloned.1.call-update) | async-done | bytes 4194320 | tf_op jit(solution)/shard_map/all_gather | solution.py:67
  162.1 6.4 %copy.18 = bf16[8192,256]{0,1:T(8,128)(2,1)} copy(bf16[8192,256]{1,0:T(8,128)(2,1)} %all-gather.5.cloned.1.call-done) | data formatting | bytes 8388608
  168.5 0.1 broadcast_in_dim.40
  168.6 12.4 %while.18 = (s32[]{:T(128)}, f32[2,1024]{1,0:T(2,128)S(1)}, f32[2,1024]{1,0:T(2,128)S(1)}, f32[2,1024,128]{2,1,0:T(8,128)S(1)}, s32[]{:T(128)}, /*index=5*/bf16[...) while((s32[]{:T(128)}, f32[2,1024]{1,0:T(2,128)S(1)}, ...), condition=%wide.region_9.10_spmd.clone, body=%wide.region_4.9_spmd.clone.sunk | while | flops 1115166720 | bytes 35352928 | solution.py:114
  168.6 11.9 %conditional.3 = ((f32[2,1024]{1,0:T(2,128)S(1)}, f32[2,1024]{1,0:T(2,128)S(1)}, f32[2,1024,128]{2,1,0:T(8,128)S(1)})) conditional(s32[]{:T(128)} %convert_element_type.57, (f32[2,1024]{1,0:T(2,128)S(1)}, f32[2,1024]{1,0:T(2,128)S(1)}, f32[2,1024,128]{2,1,0:T(8,128)S(1)}) %tuple.78, (s32[]{:T(128)}, s32[1024]{0:T(1024)S(1)}, s32[]{:T(128)}, ...), branch_computations={%region_5.5_spmd, %region_6.8_spmd} | conditional | flops 1115166720 | bytes 35348560 | solution.py:112
  168.7 1.3 constant_dynamic-slice_fusion
  170.0 0.7 broadcast_compare_fusion
  170.6 2.6 fusion.6
  173.3 3.0 fusion.5
  176.3 4.2 %fusion.10 = f32[2,1024,128]{2,1,0:T(8,128)S(1)} fusion(bf16[1024,2,128]{0,2,1:T(8,128)(2,1)S(1)} %bitcast.65, f32[2,1024,1024]{2,1,0:T(8,128)S(1)} %get-tuple-element.336, f32[2,1024]{1,0:T(2,128)S(1)} %max.2, f32[2,1024]{1,0:T(2,128)S(1)} %dynamic-slice_bitcast_fusion, f32[2,1024]{1,0:T(2,128)S(1)} %get-tuple-element.230, ...), kind=kOutput, calls=%fused_computation.10 | convolution fusion | flops 552075264 | bytes 12091392 | tf_op jit(solution)/shard_map/while/body/eval_jaxpr/cond/branch_1_fun/hqk,khd->hqd/dot_general | solution.py:100
  181.0 0.3 copy.19
  181.3 0.1 divide_convert_fusion
  181.4 0.0 copy-start.1
  181.4 7.1 %add_convert_fusion = bf16[1024,2048]{1,0:T(8,128)(2,1)} fusion(f32[1024,2048]{1,0:T(8,128)} %fusion.51, bf16[1024,256]{0,1:T(8,128)(2,1)S(1)} %bitcast.67, bf16[2048,2048]{1,0:T(8,128)(2,1)} %param.23, s32[]{:T(128)S(6)} %select_n.19), kind=kOutput, calls=%fused_computation.21 | convolution fusion | flops 1077936128 | bytes 14155780 | tf_op jit(solution)/shard_map/dot_general | solution.py:123
  188.5 0.0 reduce-scatter.2.cloned.1.call-update
  188.5 126.7 %reduce-scatter.2.cloned.1.call-done = bf16[256,2048]{1,0:T(8,128)(2,1)} async-done(((bf16[1024,2048]{1,0:T(8,128)(2,1)}), bf16[256,2048]{1,0:T(8,128)(2,1)}) %reduce-scatter.2.cloned.1.call-update) | async-done | bytes 1048592 | tf_op jit(solution)/shard_map/reduce_scatter | solution.py:122
  315.2 0.0 copy-done.1
  (27 shorter events, 0.2 us)
Async XLA Ops:
  6.5 1.2 copy-start
  6.5 10.3 %copy-start.6 = (bf16[2048,256]{1,0:T(8,128)(2,1)S(1)}, bf16[2048,256]{1,0:T(8,128)(2,1)}, u32[]{:S(2)}) copy-start(bf16[2048,256]{1,0:T(8,128)(2,1)} %param.19) | copy-start | bytes 3145732
  6.5 81.9 %all-gather.3.cloned.1.call-start = ((), (), s32[]{:S(2)}) async-start(), calls=%async_computation.1 | async-start | bytes 4718592 | tf_op jit(solution)/shard_map/all_gather | solution.py:66
  12.0 8.4 %copy-start.7 = (bf16[2048,256]{1,0:T(8,128)(2,1)S(1)}, bf16[2048,256]{1,0:T(8,128)(2,1)}, u32[]{:S(2)}) copy-start(bf16[2048,256]{1,0:T(8,128)(2,1)} %param.18) | copy-start | bytes 3145732
  12.0 150.1 %all-gather.5.cloned.1.call-start = ((), (), s32[]{:S(2)}) async-start(), calls=%async_computation.2 | async-start | bytes 4718592 | tf_op jit(solution)/shard_map/all_gather | solution.py:67
  16.7 298.5 %reduce-scatter.2.cloned.1.call-start = ((), (), s32[]{:S(2)}) async-start(), calls=%async_computation.3 | async-start | bytes 5242880 | tf_op jit(solution)/shard_map/reduce_scatter | solution.py:122
  16.8 3.6 %copy-start.5 = (bf16[1024,2048]{1,0:T(8,128)(2,1)S(1)}, bf16[1024,2048]{1,0:T(8,128)(2,1)}, u32[]{:S(2)}) copy-start(bf16[1024,2048]{1,0:T(8,128)(2,1)} %param.14) | copy-start | bytes 12582916
  21.7 9.0 %copy-start.3 = (f32[31,256]{1,0:T(8,128)S(1)}, f32[31,256]{1,0:T(8,128)}, u32[]{:S(2)}) copy-start(f32[31,256]{1,0:T(8,128)} %param.20) | copy-start | bytes 95236
  21.7 9.1 %copy-start.2 = (f32[1024,2]{0,1:T(2,128)S(1)}, f32[1024,2]{0,1:T(2,128)}, u32[]{:S(2)}) copy-start(f32[1024,2]{0,1:T(2,128)} %param.22) | copy-start | bytes 24580
  21.7 40.9 %collective-permute-start = (bf16[30,256]{1,0:T(8,128)(2,1)S(1)}, bf16[30,256]{1,0:T(8,128)(2,1)S(1)}, u32[]{:S(2)}, u32[]{:S(2)}) collective-permute-start(bf16[30,256]{1,0:T(8,128)(2,1)S(1)} %slice.252), channel_id=1, source_target_pairs={{0,4},{4,8},{8,12},{12,16},{16,20},{20,24},{24,28},{1,5},{5,9},{9,... | collective-permute-start | bytes 46088 | tf_op jit(solution)/shard_map/ppermute | solution.py:14
  62.7 17.4 %copy-start.4 = (f32[256]{0:T(256)S(1)}, f32[256]{0:T(256)}, u32[]{:S(2)}) copy-start(f32[256]{0:T(256)} %param.21) | copy-start | bytes 3076
  181.4 133.8 %copy-start.1 = (bf16[2048,256]{1,0:T(8,128)(2,1)S(1)}, bf16[2048,256]{1,0:T(8,128)(2,1)}, u32[]{:S(2)}) copy-start(bf16[2048,256]{1,0:T(8,128)(2,1)} %param.16) | copy-start | bytes 3145732
Sparse Core Ops, SparseCore 0:
  12.1 76.2 all-gather.2
  90.6 71.4 all-gather.4
  188.6 126.5 reduce-scatter.1
where the time goes:
time: 322 us
  waiting for transfers between devices  196 us (61%)
  blocking collectives  44.5 us (14%)
  matrix products  37.3 us (12%)
  local copies, waits for them, and re-layouts  16.1 us (5%)
  between operations  13.3 us (4%)
  other arithmetic  8.6 us (3%)
  starting transfers between devices  4.96 us (2%)
    reduce_scatter x1, waiting for transfers between devices, on_device(): lax.psum_scatter((projected + jnp.dot(attn_rows, attn_weight, preferred_e...  127 us
    all_gather x1, waiting for transfers between devices, on_device(): piece_values = lax.all_gather(value_rows, 'sp', axis=0, tiled=True)  67.2 us
    all_gather x1, blocking collectives, on_device(): gates_all = lax.all_gather(log_forget, 'sp', axis=0, tiled=True)  31.8 us
    unnamed x19, local copies, waits for them, and re-layouts  14.3 us
    dot_general x1, matrix products, on_device(): jnp.dot(attn_rows, attn_weight, preferred_element_type=jnp.float32)  7.05 us
    psum x1, blocking collectives, on_device(): lax.psum(jnp.sum(centered * centered, axis=1), 'tp') / total_channels  6.63 us
  transfers between devices with their start and end apart: 4, of which 3 were waited for; matrix products, arithmetic and copies ran while one was open for 10% of the time, Pallas kernels for 0%

commit v1 on v0

--- a/solution.py
+++ b/solution.py
@@ -63,8 +63,10 @@
         jnp.zeros((heads_here, tok_rows), jnp.float32),
         jnp.zeros((heads_here, tok_rows, HEAD_DIM), jnp.float32),
     )
-    piece_keys = lax.all_gather(key_rows, "sp", axis=0, tiled=True)
-    piece_values = lax.all_gather(value_rows, "sp", axis=0, tiled=True)
+    wide_out = jax.lax.all_gather(
+        jnp.concatenate([key_rows, value_rows], axis=1), axis_name="sp", axis=0, tiled=True
+    )
+    piece_keys, piece_values = jnp.split(wide_out, [key_rows.shape[1]], axis=1)
     block_rows = math.gcd(piece_keys.shape[0], tok_rows)
     shards = piece_keys.shape[0] // block_rows
     key_iota = jnp.arange(block_rows, dtype=jnp.int32)

time: 322 us -> 301 us (0.935)
  waiting for transfers between devices: 196 us -> 184 us
  local copies, waits for them, and re-layouts: 16.1 us -> 9.2 us
  matrix products: 37.3 us -> 33.8 us
    unnamed x19 -> x21, local copies, waits for them, and re-layouts: 14.3 us -> 1.54 us
    all_gather x2 -> x1, waiting for transfers between devices: 69.7 us -> 57.6 us  [on_device(): jax.lax.all_gather(jnp.concatenate([key_rows, value_rows], axis=1), axis_...]
    split x0 -> x1, local copies, waits for them, and re-layouts: none -> 5.9 us  [on_device(): piece_keys, piece_values = jnp.split(wide_out, [key_rows.shape[1]], axis=1)]
    dot_general x1, matrix products: 4.63 us -> 1.29 us  [on_device(): jnp.dot(inputs, w_value, preferred_element_type=jnp.float32)]
  transfers between devices with their start and end apart: 4 -> 3, of which waited for: 3 -> 2; matrix products, arithmetic and copies ran while one was open for 10% -> 7% of each run, Pallas kernels for 0% -> 0%
where the time goes in v1:
time: 301 us
  waiting for transfers between devices  184 us (61%)
  blocking collectives  45.1 us (15%)
  matrix products  33.8 us (11%)
  between operations  13.7 us (5%)
  other arithmetic  9.64 us (3%)
  local copies, waits for them, and re-layouts  9.2 us (3%)
  starting transfers between devices  4.91 us (2%)
    reduce_scatter x1, waiting for transfers between devices, on_device(): lax.psum_scatter((projected + jnp.dot(attn_rows, attn_weight, preferred_e...  126 us
    all_gather x1, waiting for transfers between devices, on_device(): jax.lax.all_gather(jnp.concatenate([key_rows, value_rows], axis=1), axis_...  57.6 us
    all_gather x1, blocking collectives, on_device(): gates_all = lax.all_gather(log_forget, 'sp', axis=0, tiled=True)  32.5 us
    dot_general x1, matrix products, on_device(): jnp.dot(attn_rows, attn_weight, preferred_element_type=jnp.float32)  7.05 us
    psum x1, blocking collectives, on_device(): lax.psum(jnp.sum(centered * centered, axis=1), 'tp') / total_channels  6.93 us
  transfers between devices with their start and end apart: 3, of which 2 were waited for; matrix products, arithmetic and copies ran while one was open for 7% of the time, Pallas kernels for 0%

profile of v1, /device:TPU:0, one launch (start us, length us, event | category | flops | bytes accessed | tf_op | source)
XLA Modules:
  0.0 300.7 jit_solution(1171972995764183568)
XLA Ops:
  6.5 0.0 copy-start
  6.5 0.0 copy-start.7
  6.5 0.0 all-gather.2.cloned.1.call-start
  6.5 1.2 copy-done
  7.8 0.0 copy-start.5
  7.8 3.6 %convolution_convert_fusion.2 = bf16[1024,256]{0,1:T(8,128)(2,1)S(1)} fusion(bf16[1024,2048]{1,0:T(8,128)(2,1)} %param.14, bf16[2048,256]{1,0:T(8,128)(2,1)S(1)} %copy-done), kind=kOutput, calls=%fused_computation.30 | convolution fusion | flops 1074003968 | bytes 5767168 | tf_op jit(solution)/shard_map/dot_general | solution.py:54
  11.4 0.0 copy-done.7
  11.4 0.0 copy-done.5
  11.4 0.0 copy-start.8
  11.4 1.3 convolution_convert_fusion.1
  12.7 0.0 copy-start.9
  12.7 1.0 pad_maximum_fusion
  13.8 0.0 all-gather.2.cloned.1.call-update
  13.8 0.0 reduce-scatter.2.cloned.1.call-start
  13.9 0.0 copy-done.8
  13.9 0.0 copy-start.6
  13.9 3.6 %fusion.18 = f32[1024,256]{1,0:T(8,128)S(1)} fusion(bf16[1024,2048]{1,0:T(8,128)(2,1)} %param.14, bf16[2048,256]{1,0:T(8,128)(2,1)S(1)} %copy-done.8), kind=kOutput, calls=%fused_computation.26 | convolution fusion | flops 1074528256 | bytes 6291456 | tf_op jit(solution)/shard_map/dot_general | solution.py:39
  17.5 0.0 copy-done.9
  17.5 0.0 copy-done.6
  17.5 1.3 fusion.19
  18.8 0.0 copy-start.3
  18.8 0.0 copy-start.2
  18.8 4.9 %collective-permute-start = (bf16[30,256]{1,0:T(8,128)(2,1)S(1)}, bf16[30,256]{1,0:T(8,128)(2,1)S(1)}, u32[]{:S(2)}, u32[]{:S(2)}) collective-permute-start(bf16[30,256]{1,0:T(8,128)(2,1)S(1)} %slice.252), channel_id=1, source_target_pairs={{0,4},{4,8},{8,12},{12,16},{16,20},{20,24},{24,28},{1,5},{5,9},{9,... | collective-permute-start | bytes 46088 | tf_op jit(solution)/shard_map/ppermute | solution.py:14
  23.7 4.3 %convolution_convert_fusion = bf16[1024,256]{0,1:T(8,128)(2,1)S(1)} fusion(bf16[1024,2048]{1,0:T(8,128)(2,1)} %param.14, bf16[2048,256]{1,0:T(8,128)(2,1)} %param.15), kind=kOutput, calls=%fused_computation.28 | convolution fusion | flops 1074003968 | bytes 5767168 | tf_op jit(solution)/shard_map/dot_general | solution.py:53
  28.0 0.3 copy.18
  28.3 0.0 copy-done.3
  28.3 0.0 copy-done.2
  28.3 32.5 %all_gather.7 = f32[8192,2]{0,1:T(2,128)S(1)} all-gather(f32[1024,2]{0,1:T(2,128)S(1)} %copy-done.2), channel_id=1, replica_groups=mesh['sp'=8,'tp'=4] {'sp'}, dimensions={0}, use_global_device_ids=true | all-gather | bytes 73728 | tf_op jit(solution)/shard_map/all_gather | solution.py:58
  60.9 0.0 collective-permute-done
  60.9 0.1 maximum_convert_fusion
  61.0 0.0 copy-start.4
  61.0 4.3 %fusion.60 = (f32[1024]{0:T(1024)S(1)}, f32[1024,256]{1,0:T(8,128)S(1)}) fusion(f32[1054,256]{1,0:T(8,128)S(1)} %maximum_convert_fusion, f32[256]{0:T(256)S(1)} %bitcast.80, f32[256]{0:T(256)S(1)} %bitcast.81, f32[256]{0:T(256)S(1)} %bitcast.83, f32[256]{0:T(256)S(1)} %bitcast.84, f32[256]{0:T(256)S(1)} %bitcast.85, f32[256]{0:T(256)S(1)} %bitcast.86, ...), kind=kLoop, calls=%fused_computation.109 | loop fusion | flops 16251904 | bytes 33590272 | tf_op jit(solution)/shard_map/reduce_sum | solution.py:47
  65.3 5.7 %psum.14 = f32[1024]{0:T(1024)S(1)} all-reduce(f32[1024]{0:T(1024)S(1)} %get-tuple-element.333), channel_id=1, replica_groups=mesh['sp'=8,'tp'=4] {'tp'}, use_global_device_ids=true, to_apply=%region_1.0 | all-reduce | flops 1024 | bytes 8192 | tf_op jit(solution)/shard_map/psum | solution.py:47
  71.0 0.4 multiply_reduce_fusion
  71.4 6.9 %psum.15 = f32[1024]{0:T(1024)S(1)} all-reduce(f32[1024]{0:T(1024)S(1)} %multiply_reduce_fusion), channel_id=1, replica_groups=mesh['sp'=8,'tp'=4] {'tp'}, use_global_device_ids=true, to_apply=%region_3.0 | all-reduce | flops 1024 | bytes 8192 | tf_op jit(solution)/shard_map/psum | solution.py:49
  78.3 0.0 copy-done.4
  78.3 5.8 %fusion.51 = f32[1024,2048]{1,0:T(8,128)} fusion(bf16[2048,2048]{1,0:T(8,128)(2,1)} %param.23, s32[]{:T(128)S(6)} %select_n.18, f32[1024,256]{1,0:T(8,128)S(1)} %get-tuple-element.334, f32[256]{0:T(256)S(1)} %copy-done.4, f32[1024]{0:T(1024)S(1)} %add_rsqrt_fusion, f32[1024]{0:T(1024)S(1)} %broadcast_multiply_fusion), kind=kOutput, calls=%fused_computation.95 | convolution fusion | flops 1075838976 | bytes 10494980 | tf_op jit(solution)/shard_map/dot_general | solution.py:123
  84.1 57.6 %all-gather.2.cloned.1.call-done = bf16[8192,512]{0,1:T(8,128)(2,1)} async-done(((bf16[1024,512]{0,1:T(8,128)(2,1)}), bf16[8192,512]{0,1:T(8,128)(2,1)}) %all-gather.2.cloned.1.call-update) | async-done | bytes 8388624 | tf_op jit(solution)/shard_map/all_gather | solution.py:66
  141.8 5.9 %fusion.62 = (bf16[8192,256]{0,1:T(8,128)(2,1)}, bf16[8192,256]{0,1:T(8,128)(2,1)}) fusion(bf16[8192,512]{0,1:T(8,128)(2,1)} %all-gather.2.cloned.1.call-done), kind=kLoop, calls=%fused_computation.110 | loop fusion | bytes 16777216 | tf_op jit(solution)/shard_map/split | solution.py:69
  147.7 0.1 broadcast_in_dim.40
  147.7 12.4 %while.18 = (s32[]{:T(128)}, f32[2,1024]{1,0:T(2,128)S(1)}, f32[2,1024]{1,0:T(2,128)S(1)}, f32[2,1024,128]{2,1,0:T(8,128)S(1)}, s32[]{:T(128)}, /*index=5*/bf16[...) while((s32[]{:T(128)}, f32[2,1024]{1,0:T(2,128)S(1)}, ...), condition=%wide.region_9.10_spmd.clone, body=%wide.region_4.9_spmd.clone.sunk | while | flops 1115166720 | bytes 35352928 | solution.py:116
  147.8 11.9 %conditional.3 = ((f32[2,1024]{1,0:T(2,128)S(1)}, f32[2,1024]{1,0:T(2,128)S(1)}, f32[2,1024,128]{2,1,0:T(8,128)S(1)})) conditional(s32[]{:T(128)} %convert_element_type.57, (f32[2,1024]{1,0:T(2,128)S(1)}, f32[2,1024]{1,0:T(2,128)S(1)}, f32[2,1024,128]{2,1,0:T(8,128)S(1)}) %tuple.79, (s32[]{:T(128)}, s32[1024]{0:T(1024)S(1)}, s32[]{:T(128)}, ...), branch_computations={%region_5.5_spmd, %region_6.8_spmd} | conditional | flops 1115166720 | bytes 35348560 | solution.py:114
  147.8 1.3 constant_dynamic-slice_fusion
  149.1 0.7 broadcast_compare_fusion
  149.8 2.6 fusion.6
  152.4 3.0 fusion.5
  155.5 4.2 %fusion.10 = f32[2,1024,128]{2,1,0:T(8,128)S(1)} fusion(bf16[1024,2,128]{0,2,1:T(8,128)(2,1)S(1)} %bitcast.65, f32[2,1024,1024]{2,1,0:T(8,128)S(1)} %get-tuple-element.336, f32[2,1024]{1,0:T(2,128)S(1)} %max.2, f32[2,1024]{1,0:T(2,128)S(1)} %dynamic-slice_bitcast_fusion, f32[2,1024]{1,0:T(2,128)S(1)} %get-tuple-element.230, ...), kind=kOutput, calls=%fused_computation.10 | convolution fusion | flops 552075264 | bytes 12091392 | tf_op jit(solution)/shard_map/while/body/eval_jaxpr/cond/branch_1_fun/hqk,khd->hqd/dot_general | solution.py:102
  160.1 0.3 copy.19
  160.5 0.1 divide_convert_fusion
  160.6 0.0 copy-start.1
  160.6 7.1 %add_convert_fusion = bf16[1024,2048]{1,0:T(8,128)(2,1)} fusion(f32[1024,2048]{1,0:T(8,128)} %fusion.51, bf16[1024,256]{0,1:T(8,128)(2,1)S(1)} %bitcast.67, bf16[2048,2048]{1,0:T(8,128)(2,1)} %param.23, s32[]{:T(128)S(6)} %select_n.19), kind=kOutput, calls=%fused_computation.21 | convolution fusion | flops 1077936128 | bytes 14155780 | tf_op jit(solution)/shard_map/dot_general | solution.py:125
  167.6 0.0 reduce-scatter.2.cloned.1.call-update
  167.7 126.2 %reduce-scatter.2.cloned.1.call-done = bf16[256,2048]{1,0:T(8,128)(2,1)} async-done(((bf16[1024,2048]{1,0:T(8,128)(2,1)}), bf16[256,2048]{1,0:T(8,128)(2,1)}) %reduce-scatter.2.cloned.1.call-update) | async-done | bytes 1048592 | tf_op jit(solution)/shard_map/reduce_scatter | solution.py:124
  293.9 0.0 copy-done.1
  (27 shorter events, 0.2 us)
Async XLA Ops:
  6.5 1.2 copy-start
  6.5 4.9 %copy-start.7 = (bf16[2048,256]{1,0:T(8,128)(2,1)S(1)}, bf16[2048,256]{1,0:T(8,128)(2,1)}, u32[]{:S(2)}) copy-start(bf16[2048,256]{1,0:T(8,128)(2,1)} %param.17) | copy-start | bytes 3145732
  6.5 135.2 %all-gather.2.cloned.1.call-start = ((), (), s32[]{:S(2)}) async-start(), calls=%async_computation.1 | async-start | bytes 9437184 | tf_op jit(solution)/shard_map/all_gather | solution.py:66
  7.8 3.6 %copy-start.5 = (bf16[1024,2048]{1,0:T(8,128)(2,1)S(1)}, bf16[1024,2048]{1,0:T(8,128)(2,1)}, u32[]{:S(2)}) copy-start(bf16[1024,2048]{1,0:T(8,128)(2,1)} %param.14) | copy-start | bytes 12582916
  11.4 2.4 copy-start.8
  12.7 4.8 %copy-start.9 = (bf16[2048,256]{1,0:T(8,128)(2,1)S(1)}, bf16[2048,256]{1,0:T(8,128)(2,1)}, u32[]{:S(2)}) copy-start(bf16[2048,256]{1,0:T(8,128)(2,1)} %param.18) | copy-start | bytes 3145732
  13.8 280.1 %reduce-scatter.2.cloned.1.call-start = ((), (), s32[]{:S(2)}) async-start(), calls=%async_computation.2 | async-start | bytes 5242880 | tf_op jit(solution)/shard_map/reduce_scatter | solution.py:124
  13.9 3.6 %copy-start.6 = (bf16[1024,2048]{1,0:T(8,128)(2,1)S(1)}, bf16[1024,2048]{1,0:T(8,128)(2,1)}, u32[]{:S(2)}) copy-start(bf16[1024,2048]{1,0:T(8,128)(2,1)} %param.14) | copy-start | bytes 12582916
  18.8 9.5 %copy-start.3 = (f32[31,256]{1,0:T(8,128)S(1)}, f32[31,256]{1,0:T(8,128)}, u32[]{:S(2)}) copy-start(f32[31,256]{1,0:T(8,128)} %param.20) | copy-start | bytes 95236
  18.8 9.5 %copy-start.2 = (f32[1024,2]{0,1:T(2,128)S(1)}, f32[1024,2]{0,1:T(2,128)}, u32[]{:S(2)}) copy-start(f32[1024,2]{0,1:T(2,128)} %param.22) | copy-start | bytes 24580
  18.8 42.0 %collective-permute-start = (bf16[30,256]{1,0:T(8,128)(2,1)S(1)}, bf16[30,256]{1,0:T(8,128)(2,1)S(1)}, u32[]{:S(2)}, u32[]{:S(2)}) collective-permute-start(bf16[30,256]{1,0:T(8,128)(2,1)S(1)} %slice.252), channel_id=1, source_target_pairs={{0,4},{4,8},{8,12},{12,16},{16,20},{20,24},{24,28},{1,5},{5,9},{9,... | collective-permute-start | bytes 46088 | tf_op jit(solution)/shard_map/ppermute | solution.py:14
  61.0 17.3 %copy-start.4 = (f32[256]{0:T(256)S(1)}, f32[256]{0:T(256)}, u32[]{:S(2)}) copy-start(f32[256]{0:T(256)} %param.21) | copy-start | bytes 3076
  160.6 133.3 %copy-start.1 = (bf16[2048,256]{1,0:T(8,128)(2,1)S(1)}, bf16[2048,256]{1,0:T(8,128)(2,1)}, u32[]{:S(2)}) copy-start(bf16[2048,256]{1,0:T(8,128)(2,1)} %param.16) | copy-start | bytes 3145732
Sparse Core Ops, SparseCore 0:
  13.9 127.7 all-gather.1
  167.8 126.0 reduce-scatter.1
